TPU v7x, 32 devices: a whole 2x2x4 slice. The times are simulated.
32 devices in a mesh: kv: 8 (over z, y), tp: 4 (over x, core).
Axes of the slice: x: 2, y: 2, z: 4, core: 2. Of those that a mesh axis runs over, the one named last changes fastest.
Arguments:
- activations: bfloat16 [64, 4096], P(None, ('kv', 'tp')), may hold values from -60 to 60
- mixer_gain: bfloat16 [4096], P(('kv', 'tp')), may hold values from 0.099609375 to 1.8984375
- channel_gain: bfloat16 [4096], P(('kv', 'tp')), may hold values from 0.099609375 to 1.8984375
- query_weight: bfloat16 [4096, 4096], P('kv', 'tp'), may hold values from -0.09375 to 0.09375
- key_weight: bfloat16 [4096, 4096], P('kv', 'tp'), may hold values from -0.09375 to 0.09375
- value_weight: bfloat16 [4096, 8192], P('kv', 'tp'), may hold values from -0.09375 to 0.09375
- gate_weight: bfloat16 [4096, 8192], P('kv', 'tp'), may hold values from -0.09375 to 0.09375
- output_weight: bfloat16 [8192, 4096], P('tp', 'kv'), may hold values from -0.1875 to 0.1875
- up_weight: bfloat16 [4096, 16384], P('kv', 'tp'), may hold values from -0.09375 to 0.09375
- down_weight: bfloat16 [16384, 4096], P('tp', 'kv'), may hold values from -0.046875 to 0.046875
- state_in: float32 [64, 16, 256, 512], P('kv', 'tp'), may hold values from -0.5 to 0.5
Outputs:
- activations_out: bfloat16 [64, 4096], P(None, ('kv', 'tp'))
- state_out: float32 [64, 16, 256, 512], P('kv', 'tp')
All inputs are finite; a program needn't handle non-finite values.
Results may differ from a plain program's by a relative error of at most 0.022.
Values may be sent and summed in bfloat16 or wider, within the bound.
A program may use at most 128 MiB of HBM per device.

v0:
```python
import jax
import jax.numpy as jnp
from jax import lax
from jax.sharding import PartitionSpec as P

D = 4096
HEADS = 16
DK = 256
DV = 512


EPS = 1e-06


def head_decays(count):
    index = jnp.arange(count, dtype=jnp.float32)
    return 1.0 - 2.0 ** (-1.0 - 6.0 * index / (count - 1))


def own_rows(values, count):
    return lax.dynamic_slice_in_dim(values, lax.axis_index("kv") * count, count, 0)


def select_rows(values, groups, first, last):
    shaped = values.reshape((groups, -1) + values.shape[1:])
    return shaped[:, first:last].reshape((-1,) + values.shape[1:])


def retain(query_sum, key_sum, value_sum, gate_sum, scale_rows, old_state, rates):
    count, heads = (old_state.shape[0], old_state.shape[1])
    query = (scale_rows * query_sum).reshape(count, heads, DK)
    key = (scale_rows * key_sum * DK ** (-0.5)).reshape(count, heads, DK)
    value = (scale_rows * value_sum).reshape(count, heads, DV)
    gate = scale_rows * gate_sum
    new_state = rates[None, :, None, None] * old_state + key[:, :, :, None] * value[:, :, None, :]
    output = jnp.einsum("shd,shde->she", query, new_state, precision=lax.Precision.HIGHEST)
    output = output * lax.rsqrt(jnp.mean(output * output, axis=2, keepdims=True) + EPS)
    mixed = (jax.nn.silu(gate) * output.reshape(count, heads * DV)).astype(jnp.bfloat16)
    return (new_state, mixed)


def per_device(
    activations,
    mixer_gain,
    channel_gain,
    query_weight,
    key_weight,
    value_weight,
    gate_weight,
    output_weight,
    up_weight,
    down_weight,
    state_in,
):
    seq_count = state_in.shape[0]
    groups = lax.axis_size("kv")
    heads_dev = state_in.shape[1]
    rates = lax.dynamic_slice_in_dim(
        head_decays(HEADS), lax.axis_index("tp") * heads_dev, heads_dev, 0
    )
    stream = activations.astype(jnp.float32)
    squares = jnp.sum(stream * stream, axis=1, keepdims=True)
    normed = (stream * mixer_gain.astype(jnp.float32)).astype(jnp.bfloat16)
    totals = lax.psum(squares, ("kv", "tp"))
    block = lax.all_gather(normed, "tp", axis=1, tiled=True)
    own_totals = own_rows(totals, seq_count)
    middle_row = max(seq_count // 2, 1)
    bounds = [(0, middle_row)] + [(middle_row, seq_count)]
    new_states = []
    mixes = []
    for first, last in bounds:
        rows = select_rows(block, groups, first, last)
        query_term = jnp.dot(rows, query_weight, preferred_element_type=jnp.float32)
        key_term = jnp.dot(rows, key_weight, preferred_element_type=jnp.float32)
        value_term = jnp.dot(rows, value_weight, preferred_element_type=jnp.float32)
        gate_term = jnp.dot(rows, gate_weight, preferred_element_type=jnp.float32)
        query_sum, key_sum, value_sum, gate_sum = (
            lax.psum_scatter(
                query_term.astype(jnp.bfloat16), "kv", scatter_dimension=0, tiled=True
            ).astype(jnp.float32),
            lax.psum_scatter(
                key_term.astype(jnp.bfloat16), "kv", scatter_dimension=0, tiled=True
            ).astype(jnp.float32),
            lax.psum_scatter(
                value_term.astype(jnp.bfloat16), "kv", scatter_dimension=0, tiled=True
            ).astype(jnp.float32),
            lax.psum_scatter(
                gate_term.astype(jnp.bfloat16), "kv", scatter_dimension=0, tiled=True
            ).astype(jnp.float32),
        )
        piece_totals = own_totals[first:last]
        scale_rows = lax.rsqrt(piece_totals / D + EPS)
        new_state, mixed = retain(
            query_sum, key_sum, value_sum, gate_sum, scale_rows, state_in[first:last], rates
        )
        new_states.append(new_state)
        mixes.append(mixed)
    state_out = jnp.concatenate(new_states, axis=0)
    mixed_all = jnp.concatenate(mixes, axis=0)
    out_terms = jnp.dot(
        lax.all_gather(mixed_all, "kv", axis=0, tiled=True),
        output_weight,
        preferred_element_type=jnp.float32,
    )
    attention = lax.psum_scatter(
        out_terms.astype(jnp.bfloat16), "tp", scatter_dimension=1, tiled=True
    ).astype(jnp.float32)
    middle = (stream + attention).astype(jnp.bfloat16)
    middle = lax.optimization_barrier(middle).astype(jnp.float32)
    middle_squares = jnp.sum(middle * middle, axis=1, keepdims=True)
    channel_normed = (middle * channel_gain.astype(jnp.float32)).astype(jnp.bfloat16)
    channel_totals = lax.psum(middle_squares, ("kv", "tp"))
    channel_block = lax.all_gather(channel_normed, "tp", axis=1, tiled=True)
    up_sum = lax.psum_scatter(
        jnp.dot(channel_block, up_weight, preferred_element_type=jnp.float32).astype(jnp.bfloat16),
        "kv",
        scatter_dimension=0,
        tiled=True,
    ).astype(jnp.float32)
    own_channel = own_rows(channel_totals, seq_count)
    lifted = lax.rsqrt(own_channel / D + EPS) * up_sum
    hidden = jnp.square(jax.nn.relu(lifted)).astype(jnp.bfloat16)
    down_terms = jnp.dot(
        lax.all_gather(hidden, "kv", axis=0, tiled=True),
        down_weight,
        preferred_element_type=jnp.float32,
    )
    lowered = lax.psum_scatter(
        down_terms.astype(jnp.bfloat16), "tp", scatter_dimension=1, tiled=True
    ).astype(jnp.float32)
    return ((middle + lowered).astype(jnp.bfloat16), state_out)


def solution(mesh):
    return jax.shard_map(
        per_device,
        mesh=mesh,
        in_specs=(
            P(None, ("kv", "tp")),
            P(("kv", "tp")),
            P(("kv", "tp")),
            P("kv", "tp"),
            P("kv", "tp"),
            P("kv", "tp"),
            P("kv", "tp"),
            P("tp", "kv"),
            P("kv", "tp"),
            P("tp", "kv"),
            P("kv", "tp", None, None),
        ),
        out_specs=(P(None, ("kv", "tp")), P("kv", "tp", None, None)),
        check_vma=False,
    )
```

profile of v0, /device:TPU:0, one launch (start us, length us, event | category | flops | bytes accessed | tf_op | source)
XLA Modules:
  0.0 324.0 jit_solution(18201089255404920594)
XLA Ops:
  7.2 0.0 copy-start
  7.2 0.0 copy-start.7
  7.2 0.0 copy-start.3
  7.2 0.0 all-reduce.11.cloned.1.call-start
  7.3 0.8 convert_element_type.100
  8.1 0.9 fusion.2
  9.0 6.2 %all_gather.12 = bf16[64,512]{1,0:T(8,128)(2,1)S(1)} all-gather(bf16[64,128]{1,0:T(8,128)(2,1)S(1)} %get-tuple-element.17), channel_id=1, replica_groups=mesh['kv'=8,'tp'=4] {'tp'}, dimensions={1}, use_global_device_ids=true | all-gather | bytes 81920 | tf_op jit(solution)/shard_map/all_gather | solution.py:65
  15.2 2.1 convolution_convert_fusion.8
  17.4 0.0 copy-done
  17.4 1.1 convolution_convert_fusion.1
  18.5 2.1 convolution_convert_fusion.10
  20.7 1.1 convolution_convert_fusion.3
  21.8 2.1 convolution_convert_fusion.7
  23.9 0.0 copy-done.3
  23.9 0.9 convolution_convert_fusion.9
  24.8 2.7 convolution_convert_fusion.2
  27.6 2.7 convolution_convert_fusion.4
  30.3 0.0 all-reduce.11.cloned.1.call-update
  30.3 0.0 reduce-scatter.10.cloned.1.call-start
  30.4 0.0 copy-done.7
  30.4 0.6 dynamic-slice
  31.6 0.1 dynamic_slice.10
  31.7 41.4 %psum.14 = f32[64,1]{0,1:T(1,128)S(1)} all-reduce(f32[64,1]{0,1:T(1,128)S(1)} %bitcast.67), channel_id=1, replica_groups=mesh['kv'=8,'tp'=4] {'kv','tp'}, use_global_device_ids=true, to_apply=%region_1.0 | all-reduce | flops 64 | bytes 512 | tf_op jit(solution)/shard_map/psum | solution.py:64
  73.1 0.1 constant_dynamic-slice_fusion
  73.2 0.1 rsqrt_bitcast_fusion.2
  73.3 35.4 %all-reduce.11.cloned.1.call-done = (bf16[32,1024]{1,0:T(8,128)(2,1)}, bf16[32,2048]{1,0:T(8,128)(2,1)}, bf16[32,1024]{1,0:T(8,128)(2,1)}, bf16[32,2048]{1,0:T(8...) async-done(((bf16[32,1024]{1,0:T(8,128)(2,1)}, bf16[32,2048]{1,0:T(8,128)(2,1)}, ...) | async-done | bytes 786448
  108.7 0.8 multiply_multiply_fusion
  109.6 0.9 convert_multiply_fusion.4
  110.6 9.6 %multiply_add_fusion.1 = (f32[4,4,256,512]{3,2,1,0:T(8,128)}, f32[4,4,256,512]{3,2,1,0:T(8,128)S(1)}) fusion(f32[8,4,256,512]{3,2,1,0:T(8,128)} %param.21, f32[4,4,512]{2,1,0:T(4,128)S(1)} %mul.207, f32[4,4,256]{2,1,0:T(4,128)S(1)} %mul.204, f32[4]{0:T(128)S(1)} %dynamic_slice.10, f32[4,4,512]{2,1,0:T(4,128)S(1)} %mul.226, f32[4,4,256]{2,1,0:T(4,128)S(1)} %mul.223), kind=kLoop, calls=%fused_computation.2 | loop fusion | flops 12582912 | bytes 33652752 | tf_op jit(solution)/shard_map/add | solution.py:35
  120.2 3.2 copy-done.2
  123.4 4.0 %fusion.16 = f32[4,4,1,512]{3,2,1,0:T(1,128)S(1)} fusion(f32[4,4,256,1]{2,3,1,0:T(1,128)S(1)} %reshape.63, f32[4,4,256,512]{3,2,1,0:T(8,128)S(1)} %get-tuple-element.11), kind=kOutput, calls=%fused_computation.57 | convolution fusion | flops 25165824 | bytes 8437760 | tf_op jit(solution)/shard_map/shd,shde->she/dot_general | solution.py:36
  127.4 0.1 fusion.8
  127.5 0.1 fusion.9
  127.7 7.4 %fusion.15 = f32[4,4,1,512]{3,2,1,0:T(1,128)S(1)} fusion(f32[4,4,256,1]{2,3,1,0:T(1,128)S(1)} %reshape.61, f32[4,4,256,512]{3,2,1,0:T(8,128)} %get-tuple-element.10), kind=kOutput, calls=%fused_computation.56 | convolution fusion | flops 25165824 | bytes 8437760 | tf_op jit(solution)/shard_map/shd,shde->she/dot_general | solution.py:36
  135.1 0.1 fusion.10
  135.2 0.1 fusion.11
  135.3 0.9 fusion.12
  136.2 0.9 fusion.13
  137.1 30.7 %all_gather.13 = bf16[64,2048]{1,0:T(8,128)(2,1)S(1)} all-gather(bf16[8,2048]{1,0:T(8,128)(2,1)S(1)} %pad_maximum_fusion.1), channel_id=1, replica_groups=mesh['kv'=8,'tp'=4] {'kv'}, dimensions={0}, use_global_device_ids=true | all-gather | bytes 294912 | tf_op jit(solution)/shard_map/all_gather | solution.py:101
  167.8 0.5 convolution_convert_fusion.6
  168.3 0.8 copy.17
  169.1 0.0 reduce-scatter.10.cloned.1.call-update
  169.1 0.0 reduce-scatter.8.cloned.1.call-start
  169.1 0.0 copy-done.6
  169.2 18.9 %reduce-scatter.10.cloned.1.call-done = bf16[128,64]{1,0:T(8,128)(2,1)} async-done(((bf16[512,64]{1,0:T(8,128)(2,1)}), bf16[128,64]{1,0:T(8,128)(2,1)}) %reduce-scatter.10.cloned.1.call-update) | async-done | bytes 16400
  188.1 0.8 copy.18
  189.0 0.1 fusion.5
  189.1 5.3 %all_gather.14 = bf16[64,512]{1,0:T(8,128)(2,1)S(1)} all-gather(bf16[64,128]{1,0:T(8,128)(2,1)S(1)} %get-tuple-element.15), channel_id=1, replica_groups=mesh['kv'=8,'tp'=4] {'tp'}, dimensions={1}, use_global_device_ids=true | all-gather | bytes 81920 | tf_op jit(solution)/shard_map/all_gather | solution.py:113
  194.3 3.8 %convolution_convert_fusion = bf16[64,4096]{1,0:T(8,128)(2,1)} fusion(bf16[64,512]{1,0:T(8,128)(2,1)S(1)} %all_gather.14, bf16[512,4096]{1,0:T(8,128)(2,1)} %param.19), kind=kOutput, calls=%fused_computation.3 | convolution fusion | flops 268697600 | bytes 4784128 | tf_op jit(solution)/shard_map/dot_general | solution.py:115
  198.2 0.0 reduce-scatter.8.cloned.1.call-update
  198.2 0.0 reduce-scatter.12.cloned.1.call-start
  198.2 39.4 %psum.15 = f32[64,1]{0,1:T(1,128)S(1)} all-reduce(f32[64,1]{0,1:T(1,128)S(1)} %bitcast.68), channel_id=1, replica_groups=mesh['kv'=8,'tp'=4] {'kv','tp'}, use_global_device_ids=true, to_apply=%region_14.15 | all-reduce | flops 64 | bytes 512 | tf_op jit(solution)/shard_map/psum | solution.py:112
  237.7 0.1 rsqrt_bitcast_fusion
  237.8 23.3 %reduce-scatter.8.cloned.1.call-done = bf16[8,4096]{1,0:T(8,128)(2,1)} async-done(((bf16[64,4096]{1,0:T(8,128)(2,1)}), bf16[8,4096]{1,0:T(8,128)(2,1)}) %reduce-scatter.8.cloned.1.call-update) | async-done | bytes 65552 | tf_op jit(solution)/shard_map/reduce_scatter | solution.py:114
  261.1 0.9 multiply_convert_fusion
  262.0 31.4 %all_gather.15 = bf16[64,4096]{1,0:T(8,128)(2,1)S(1)} all-gather(bf16[8,4096]{1,0:T(8,128)(2,1)S(1)} %multiply_convert_fusion), channel_id=1, replica_groups=mesh['kv'=8,'tp'=4] {'kv'}, dimensions={0}, use_global_device_ids=true | all-gather | bytes 589824 | tf_op jit(solution)/shard_map/all_gather | solution.py:124
  293.4 3.0 convolution_convert_fusion.5
  296.5 0.7 copy.19
  297.2 0.0 reduce-scatter.12.cloned.1.call-update
  297.2 0.0 copy-start.1
  297.2 12.0 %pad_maximum_fusion = f32[8,4,256,512]{3,2,1,0:T(8,128)} fusion(f32[4,4,256,512]{3,2,1,0:T(8,128)} %copy-done.2, f32[4,4,256,512]{3,2,1,0:T(8,128)} %get-tuple-element.10), kind=kLoop, calls=%fused_computation | loop fusion | flops 4194304 | bytes 33554432 | tf_op jit(solution)/shard_map/concatenate | solution.py:98
  309.2 6.8 %reduce-scatter.12.cloned.1.call-done = bf16[128,64]{1,0:T(8,128)(2,1)} async-done(((bf16[512,64]{1,0:T(8,128)(2,1)}), bf16[128,64]{1,0:T(8,128)(2,1)}) %reduce-scatter.12.cloned.1.call-update) | async-done | bytes 16400
  316.0 0.8 copy.20
  316.9 0.6 fusion.7
  (24 shorter events, 0.3 us)
Async XLA Ops:
  7.2 10.2 %copy-start = (bf16[512,2048]{1,0:T(8,128)(2,1)S(1)}, bf16[512,2048]{1,0:T(8,128)(2,1)}, u32[]{:S(2)}) copy-start(bf16[512,2048]{1,0:T(8,128)(2,1)} %param.16) | copy-start | bytes 6291460
  7.2 23.2 %copy-start.7 = (u32[32]{0:T(128)S(1)}, u32[32]{0:T(128)}, u32[]{:S(2)}) copy-start(u32[32]{0:T(128)} %constant.55) | copy-start | bytes 388
  7.2 16.7 %copy-start.3 = (bf16[512,1024]{1,0:T(8,128)(2,1)S(1)}, bf16[512,1024]{1,0:T(8,128)(2,1)}, u32[]{:S(2)}) copy-start(bf16[512,1024]{1,0:T(8,128)(2,1)} %param.15) | copy-start | bytes 3145732
  7.2 101.5 %all-reduce.11.cloned.1.call-start = ((), (), s32[]{:S(2)}) async-start(), calls=%async_computation.6 | async-start | bytes 1572864
  30.3 157.8 %reduce-scatter.10.cloned.1.call-start = ((), (), s32[]{:S(2)}) async-start(), calls=%async_computation.4 | async-start | bytes 163840
  120.2 3.2 copy-start.2
  123.4 44.5 %copy-start.4 = (bf16[2048,512]{1,0:T(8,128)(2,1)S(1)}, bf16[2048,512]{1,0:T(8,128)(2,1)}, u32[]{:S(2)}) copy-start(bf16[2048,512]{1,0:T(8,128)(2,1)} %param.18) | copy-start | bytes 6291460
  123.4 45.8 %copy-start.6 = (bf16[128]{0:T(256)(128)(2,1)S(1)}, bf16[128]{0:T(256)(128)(2,1)}, u32[]{:S(2)}) copy-start(bf16[128]{0:T(256)(128)(2,1)} %param.13) | copy-start | bytes 772
  123.4 65.6 %copy-start.5 = (bf16[64,128]{1,0:T(8,128)(2,1)S(1)}, bf16[64,128]{1,0:T(8,128)(2,1)}, u32[]{:S(2)}) copy-start(bf16[64,128]{1,0:T(8,128)(2,1)} %param.11) | copy-start | bytes 49156
  169.1 92.0 %reduce-scatter.8.cloned.1.call-start = ((), (), s32[]{:S(2)}) async-start(), calls=%async_computation.3 | async-start | bytes 589824 | tf_op jit(solution)/shard_map/reduce_scatter | solution.py:114
  198.2 117.8 %reduce-scatter.12.cloned.1.call-start = ((), (), s32[]{:S(2)}) async-start(), calls=%async_computation.5 | async-start | bytes 163840
  297.2 20.3 %copy-start.1 = (bf16[512,2048]{1,0:T(8,128)(2,1)S(1)}, bf16[512,2048]{1,0:T(8,128)(2,1)}, u32[]{:S(2)}) copy-start(bf16[512,2048]{1,0:T(8,128)(2,1)} %param.16) | copy-start | bytes 6291460
Sparse Core Ops, SparseCore 0:
  30.4 78.2 all-reduce.10
  169.2 18.8 reduce-scatter.9
  198.3 62.7 reduce-scatter.7
  297.3 18.6 reduce-scatter.11
where the time goes:
time: 325 us; the launch traced here: 324 us
  blocking collectives  155 us (48%)
  waiting for transfers between devices  84.5 us (26%)
  matrix products  33.8 us (10%)
  other arithmetic  29 us (9%)
  between operations  14.6 us (4%)
  local copies, waits for them, and re-layouts  7.43 us (2%)
    unnamed x7, waiting for transfers between devices  61.2 us
    psum x1, blocking collectives, per_device(): totals = lax.psum(squares, ('kv', 'tp'))  41.4 us
    psum x1, blocking collectives, per_device(): channel_totals = lax.psum(middle_squares, ('kv', 'tp'))  39.4 us
    all_gather x1, blocking collectives, per_device(): lax.all_gather(hidden, 'kv', axis=0, tiled=True)  31.4 us
    all_gather x1, blocking collectives, per_device(): lax.all_gather(mixed_all, 'kv', axis=0, tiled=True)  30.7 us
    reduce_scatter x1, waiting for transfers between devices, per_device(): lax.psum_scatter(jnp.dot(channel_block, up_weight, preferred_element_type...  23.3 us
    concatenate x1, other arithmetic, per_device(): state_out = jnp.concatenate(new_states, axis=0)  12 us
    dot_general x2, matrix products, retain(): jnp.einsum('shd,shde->she', query, new_state, precision=lax.Precision.HIG...  11.5 us
  transfers between devices with their start and end apart: 4, of which 4 were waited for; matrix products, arithmetic and copies ran while one was open for 4% of the time, Pallas kernels for 0%

commit v1 on v0

v1 whole, which is shorter than its diff:
```python
import functools

import jax
import jax.numpy as jnp
from jax import lax
from jax.experimental import pallas as pl
from jax.experimental.pallas import tpu as pltpu
from jax.sharding import PartitionSpec as P

HEADS = 16
EPS = 1e-06
MESH = pl.DeviceIdType.MESH
F32 = jnp.float32
BF16 = jnp.bfloat16
DMA = pltpu.SemaphoreType.DMA
PAIR = 2
LAG = 2


def head_decays(count):
    index = jnp.arange(count, dtype=jnp.float32)
    return 1.0 - 2.0 ** (-1.0 - 6.0 * index / (count - 1))


def put(src, dst, send_sem, recv_sem, where):
    copy = pltpu.make_async_remote_copy(
        src_ref=src,
        dst_ref=dst,
        send_sem=send_sem,
        recv_sem=recv_sem,
        device_id=where,
        device_id_type=MESH,
    )
    copy.start()
    return copy


def greet(kv, tp, n_kv, n_tp):
    barrier = pltpu.get_barrier_semaphore()
    for d in range(1, n_tp):
        pl.semaphore_signal(
            barrier, inc=1, device_id={"tp": lax.rem(tp + d, n_tp)}, device_id_type=MESH
        )
    for d in range(1, n_kv):
        pl.semaphore_signal(
            barrier, inc=1, device_id={"kv": lax.rem(kv + d, n_kv)}, device_id_type=MESH
        )
    pl.semaphore_wait(barrier, n_tp + n_kv - 2)


def tp_gather(buf, tp, n_tp, sems):
    return [
        put(
            buf.at[tp],
            buf.at[tp],
            sems.at[0, d - 1],
            sems.at[1, d - 1],
            {"tp": lax.rem(tp + d, n_tp)},
        )
        for d in range(1, n_tp)
    ]


def tp_scatter(src, dst, tp, n_tp, sems):
    copies = []
    for d in range(1, n_tp):
        peer = lax.rem(tp + d, n_tp)
        copies.append(
            put(src.at[peer], dst.at[d - 1], sems.at[0, d - 1], sems.at[1, d - 1], {"tp": peer})
        )
    return copies


def kv_scatter_small(src, dst, kv, n_kv, sems):
    copies = []
    for d in range(1, n_kv):
        peer = lax.rem(kv + d, n_kv)
        copies.append(
            put(src.at[peer], dst.at[d - 1], sems.at[0, d - 1], sems.at[1, d - 1], {"kv": peer})
        )
    return copies


def own_square_total(squares, sq_src, sq_dst, kv, n_kv, rows, sems):
    for g in range(n_kv):
        sq_src[g] = jnp.broadcast_to(squares[g * rows : (g + 1) * rows], sq_src.shape[1:])
    copies = kv_scatter_small(sq_src, sq_dst, kv, n_kv, sems)

    def finish():
        total = sq_src[kv]
        for d, copy in enumerate(copies):
            copy.wait_recv()
            total = total + sq_dst[d]
        return total[:, :1]

    return copies, finish


class PairScatter:
    def __init__(self, kv, n_kv, rows, part, got, summed, got2, sem_a, sem_b):
        self.n_z = n_kv // PAIR
        self.z, self.y = lax.div(kv, PAIR), lax.rem(kv, PAIR)
        self.rows = rows
        self.part, self.got, self.summed, self.got2 = part, got, summed, got2
        self.sem_a, self.sem_b = sem_a, sem_b
        self.first, self.second = {}, {}

    def start(self, p, value):
        rows = self.rows
        for z in range(self.n_z):
            for y in range(PAIR):
                at = (z * PAIR + y) * rows
                self.part[p, y, z] = value[at : at + rows].astype(BF16)
        other = 1 - self.y
        self.first[p] = put(
            self.part.at[p, other],
            self.got.at[p],
            self.sem_a.at[0, p],
            self.sem_a.at[1, p],
            {"kv": self.z * PAIR + other},
        )

    def middle(self, p):
        self.first[p].wait_recv()
        self.summed[p] = (self.part[p, self.y].astype(F32) + self.got[p].astype(F32)).astype(BF16)
        copies = []
        for d in range(1, self.n_z):
            peer = lax.rem(self.z + d, self.n_z)
            copies.append(
                put(
                    self.summed.at[p, peer],
                    self.got2.at[p, d - 1],
                    self.sem_b.at[0, p, d - 1],
                    self.sem_b.at[1, p, d - 1],
                    {"kv": peer * PAIR + self.y},
                )
            )
        self.second[p] = copies

    def finish(self, p):
        total = self.summed[p, self.z].astype(F32)
        for d, copy in enumerate(self.second[p]):
            copy.wait_recv()
            total = total + self.got2[p, d].astype(F32)
        return total

    def drain(self):
        for p in self.first:
            self.first[p].wait_send()
            for copy in self.second[p]:
                copy.wait_send()


class PairGather:
    def __init__(self, kv, n_kv, buf, sem_z, sem_y):
        self.n_z = n_kv // PAIR
        self.z, self.y = lax.div(kv, PAIR), lax.rem(kv, PAIR)
        self.buf, self.sem_z, self.sem_y = buf, sem_z, sem_y
        self.along, self.across = {}, {}

    def forward(self, p, d):
        z = lax.rem(self.z - d + self.n_z, self.n_z)
        self.across[p].append(
            put(
                self.buf.at[p, z, self.y],
                self.buf.at[p, z, self.y],
                self.sem_y.at[0, p, d],
                self.sem_y.at[1, p, d],
                {"kv": self.z * PAIR + 1 - self.y},
            )
        )

    def start(self, p):
        own = self.buf.at[p, self.z, self.y]
        self.along[p], self.across[p] = [], []
        for d in range(1, self.n_z):
            peer = lax.rem(self.z + d, self.n_z)
            self.along[p].append(
                put(
                    own,
                    own,
                    self.sem_z.at[0, p, d - 1],
                    self.sem_z.at[1, p, d - 1],
                    {"kv": peer * PAIR + self.y},
                )
            )
        self.forward(p, 0)

    def relay(self, p):
        for d, copy in enumerate(self.along[p]):
            copy.wait_recv()
            self.forward(p, d + 1)

    def finish(self, p):
        for copy in self.across[p]:
            copy.wait_recv()
        blocks = [
            self.buf[p, z, y].astype(F32) for z in range(self.n_z) for y in range(PAIR)
        ]
        return jnp.concatenate(blocks, axis=0).astype(BF16)

    def drain(self):
        for p in self.along:
            for copy in self.along[p] + self.across[p]:
                copy.wait_send()


def project_kernel(
    sizes,
    x_ref,
    gain_ref,
    *refs,
):
    n_kv, n_tp, rows, width, counts, dim = sizes
    weights, refs = refs[:4], refs[4:]
    outs, refs = refs[:4], refs[4:]
    (xs, gains, w, part, got, summed, got2, sq_src, sq_dst) = refs[:9]
    (w_sem, x_sem, g_sem, sq_sem, sem_a, sem_b) = refs[9:]
    kv, tp = lax.axis_index("kv"), lax.axis_index("tp")
    pieces = [(i, j) for i, count in enumerate(counts) for j in range(count)]
    loads = []
    for p, (i, j) in enumerate(pieces):
        load = pltpu.make_async_copy(
            weights[i].at[:, pl.ds(j * width, width)], w.at[p], w_sem.at[p]
        )
        load.start()
        loads.append(load)
    xs[tp] = x_ref[...]
    gains[tp] = jnp.broadcast_to(gain_ref[...].astype(F32), gains.shape[1:])
    greet(kv, tp, n_kv, n_tp)
    x_copies = tp_gather(xs, tp, n_tp, x_sem)
    g_copies = tp_gather(gains, tp, n_tp, g_sem)
    for copy in x_copies + g_copies:
        copy.wait_recv()
    stream = [xs[t].astype(F32) for t in range(n_tp)]
    normed = jnp.concatenate(
        [(stream[t] * gains[t][:1]).astype(BF16) for t in range(n_tp)], axis=1
    )
    squares = sum(jnp.sum(s * s, axis=1, keepdims=True) for s in stream)
    sq_copies, sq_total = own_square_total(squares, sq_src, sq_dst, kv, n_kv, rows, sq_sem)
    scatter = PairScatter(kv, n_kv, rows, part, got, summed, got2, sem_a, sem_b)
    for p in range(len(pieces)):
        loads[p].wait()
        scatter.start(p, jnp.dot(normed, w[p], preferred_element_type=F32))
        if p >= LAG:
            scatter.middle(p - LAG)
    for p in range(max(len(pieces) - LAG, 0), len(pieces)):
        scatter.middle(p)
    scale = lax.rsqrt(sq_total() / dim + EPS)
    for p, (i, j) in enumerate(pieces):
        outs[i][:, j * width : (j + 1) * width] = scatter.finish(p) * scale
    scatter.drain()
    for copy in x_copies + g_copies + sq_copies:
        copy.wait_send()


def retain_kernel(heads, dk, dv, q_ref, k_ref, v_ref, g_ref, rate_ref, old_ref, new_ref, mix_ref):
    s = pl.program_id(0)
    q_row = q_ref[pl.ds(s, 1), :]
    k_row = k_ref[pl.ds(s, 1), :] * dk ** (-0.5)
    v_row = v_ref[pl.ds(s, 1), :]
    g_row = g_ref[pl.ds(s, 1), :]
    lines = [q_row[:, h * dk : (h + 1) * dk] for h in range(heads)]
    lines += [k_row[:, h * dk : (h + 1) * dk] for h in range(heads)]
    if len(lines) % 8:
        lines.append(jnp.zeros((8 - len(lines) % 8, dk), F32))
    columns = jnp.concatenate(lines, axis=0).T
    for h in range(heads):
        value = v_row[:, h * dv : (h + 1) * dv]
        query = columns[:, h : h + 1]
        key = columns[:, heads + h : heads + h + 1]
        new = rate_ref[h] * old_ref[0, h] + key * value
        new_ref[0, h] = new
        out = jnp.sum(query * new, axis=0, keepdims=True)
        out = out * lax.rsqrt(jnp.mean(out * out, axis=1, keepdims=True) + EPS)
        gate = g_row[:, h * dv : (h + 1) * dv]
        mix_ref[pl.ds(s, 1), h * dv : (h + 1) * dv] = jax.nn.silu(gate) * out


def mix_kernel(sizes, mix_ref, x_ref, gain_ref, ow_hbm, up_hbm, down_hbm, out_ref, *refs):
    n_kv, n_tp, rows, width, count, dim = sizes
    (ow, up, down, mixes, gains, ends, got_ends, mids, part, got, summed, got2) = refs[:12]
    (sq_src, sq_dst, hid, w_sem, g_sem, mz_sem, my_sem, e_sem, m_sem, sq_sem) = refs[12:22]
    (sem_a, sem_b, hz_sem, hy_sem, f_sem) = refs[22:]
    kv, tp = lax.axis_index("kv"), lax.axis_index("tp")
    z, y = lax.div(kv, PAIR), lax.rem(kv, PAIR)
    block = x_ref.shape[1]
    ow_load = pltpu.make_async_copy(ow_hbm, ow, w_sem.at[0])
    ow_load.start()
    ups, downs = [], []
    for p in range(count):
        load = pltpu.make_async_copy(
            up_hbm.at[:, pl.ds(p * width, width)], up.at[p], w_sem.at[1 + p]
        )
        load.start()
        ups.append(load)
    for p in range(count):
        load = pltpu.make_async_copy(
            down_hbm.at[pl.ds(p * width, width), :], down.at[p], w_sem.at[1 + count + p]
        )
        load.start()
        downs.append(load)
    mixes[0, z, y] = mix_ref[...].astype(BF16)
    gains[tp] = jnp.broadcast_to(gain_ref[...].astype(F32), gains.shape[1:])
    greet(kv, tp, n_kv, n_tp)
    mix_gather = PairGather(kv, n_kv, mixes, mz_sem, my_sem)
    mix_gather.start(0)
    g_copies = tp_gather(gains, tp, n_tp, g_sem)
    mix_gather.relay(0)
    mixed = mix_gather.finish(0)
    ow_load.wait()

    def tp_sum(terms, at, sems):
        for t in range(n_tp):
            ends[at, t] = terms[:, t * block : (t + 1) * block].astype(BF16)
        copies = tp_scatter(ends.at[at], got_ends.at[at], tp, n_tp, sems)
        total = ends[at, tp].astype(F32)
        for d, copy in enumerate(copies):
            copy.wait_recv()
            total = total + got_ends[at, d].astype(F32)
        return copies, total

    e_copies, attention = tp_sum(jnp.dot(mixed, ow[...], preferred_element_type=F32), 0, e_sem)
    mids[tp] = (x_ref[...].astype(F32) + attention).astype(BF16)
    m_copies = tp_gather(mids, tp, n_tp, m_sem)
    for copy in g_copies + m_copies:
        copy.wait_recv()
    stream = [mids[t].astype(F32) for t in range(n_tp)]
    normed = jnp.concatenate(
        [(stream[t] * gains[t][:1]).astype(BF16) for t in range(n_tp)], axis=1
    )
    squares = sum(jnp.sum(s * s, axis=1, keepdims=True) for s in stream)
    sq_copies, sq_total = own_square_total(squares, sq_src, sq_dst, kv, n_kv, rows, sq_sem)
    scatter = PairScatter(kv, n_kv, rows, part, got, summed, got2, sem_a, sem_b)
    gather = PairGather(kv, n_kv, hid, hz_sem, hy_sem)
    for p in range(count):
        ups[p].wait()
        scatter.start(p, jnp.dot(normed, up[p], preferred_element_type=F32))
        if p >= LAG:
            scatter.middle(p - LAG)
    for p in range(max(count - LAG, 0), count):
        scatter.middle(p)
    scale = lax.rsqrt(sq_total() / dim + EPS)
    for p in range(count):
        lifted = scatter.finish(p) * scale
        hid[p, z, y] = jnp.square(jnp.maximum(lifted, 0.0)).astype(BF16)
        gather.start(p)
        if p >= 1:
            gather.relay(p - 1)
    gather.relay(count - 1)
    terms = None
    for p in range(count):
        hidden = gather.finish(p)
        downs[p].wait()
        term = jnp.dot(hidden, down[p], preferred_element_type=F32)
        terms = term if terms is None else terms + term
    f_copies, lowered = tp_sum(terms, 1, f_sem)
    out_ref[...] = (mids[tp].astype(F32) + lowered).astype(BF16)
    mix_gather.drain()
    gather.drain()
    scatter.drain()
    for copy in g_copies + e_copies + m_copies + sq_copies + f_copies:
        copy.wait_send()


VM = pl.BlockSpec(memory_space=pltpu.VMEM)
ANY = pl.BlockSpec(memory_space=pl.ANY)


def scatter_scratch(count, n_kv, rows, width):
    n_z = n_kv // PAIR
    return [
        pltpu.VMEM((count, PAIR, n_z, rows, width), BF16),
        pltpu.VMEM((count, n_z, rows, width), BF16),
        pltpu.VMEM((count, n_z, rows, width), BF16),
        pltpu.VMEM((count, n_z - 1, rows, width), BF16),
    ]


def fused_device(n_kv, n_tp, x, mg, cg, qw, kw, vw, gw, ow, uw, dw, state):
    seqs, heads, dk, dv = state.shape
    batch, block = x.shape
    dim = block * n_kv * n_tp
    n_z = n_kv // PAIR
    depth, width = qw.shape
    counts = tuple(m.shape[1] // width for m in (qw, kw, vw, gw))
    pieces = sum(counts)
    params = functools.partial(
        pltpu.CompilerParams, has_side_effects=True, vmem_limit_bytes=60 * 2**20
    )
    query, key, value, gate = pl.pallas_call(
        functools.partial(project_kernel, (n_kv, n_tp, seqs, width, counts, dim)),
        out_shape=[jax.ShapeDtypeStruct((seqs, m.shape[1]), F32) for m in (qw, kw, vw, gw)],
        in_specs=[VM, VM] + [ANY] * 4,
        out_specs=[VM] * 4,
        scratch_shapes=[
            pltpu.VMEM((n_tp, batch, block), BF16),
            pltpu.VMEM((n_tp, 8, block), F32),
            pltpu.VMEM((pieces, depth, width), BF16),
            *scatter_scratch(pieces, n_kv, seqs, width),
            pltpu.VMEM((n_kv, seqs, 128), F32),
            pltpu.VMEM((n_kv - 1, seqs, 128), F32),
            DMA((pieces,)),
            DMA((2, n_tp - 1)),
            DMA((2, n_tp - 1)),
            DMA((2, n_kv - 1)),
            DMA((2, pieces)),
            DMA((2, pieces, n_z - 1)),
        ],
        compiler_params=params(collective_id=0),
        name="project",
    )(x, mg.reshape(1, block), qw, kw, vw, gw)
    rates = lax.dynamic_slice_in_dim(
        head_decays(HEADS), lax.axis_index("tp") * heads, heads, 0
    )
    whole = lambda a: pl.BlockSpec(a.shape, lambda s: (0, 0))
    state_spec = pl.BlockSpec((1, heads, dk, dv), lambda s: (s, 0, 0, 0))
    new_state, mixed = pl.pallas_call(
        functools.partial(retain_kernel, heads, dk, dv),
        grid=(seqs,),
        out_shape=[
            jax.ShapeDtypeStruct(state.shape, F32),
            jax.ShapeDtypeStruct((seqs, heads * dv), F32),
        ],
        in_specs=[
            whole(query),
            whole(key),
            whole(value),
            whole(gate),
            pl.BlockSpec(memory_space=pltpu.SMEM),
            state_spec,
        ],
        out_specs=[state_spec, pl.BlockSpec((seqs, heads * dv), lambda s: (0, 0))],
        compiler_params=pltpu.CompilerParams(vmem_limit_bytes=32 * 2**20),
        name="retain",
    )(query, key, value, gate, rates, state)
    width = min(1024, uw.shape[1])
    count = uw.shape[1] // width
    out = pl.pallas_call(
        functools.partial(mix_kernel, (n_kv, n_tp, seqs, width, count, dim)),
        out_shape=jax.ShapeDtypeStruct((batch, block), BF16),
        in_specs=[VM, VM, VM, ANY, ANY, ANY],
        out_specs=VM,
        scratch_shapes=[
            pltpu.VMEM(ow.shape, BF16),
            pltpu.VMEM((count, depth, width), BF16),
            pltpu.VMEM((count, width, dw.shape[1]), BF16),
            pltpu.VMEM((1, n_z, PAIR, seqs, heads * dv), BF16),
            pltpu.VMEM((n_tp, 8, block), F32),
            pltpu.VMEM((2, n_tp, batch, block), BF16),
            pltpu.VMEM((2, n_tp - 1, batch, block), BF16),
            pltpu.VMEM((n_tp, batch, block), BF16),
            *scatter_scratch(count, n_kv, seqs, width),
            pltpu.VMEM((n_kv, seqs, 128), F32),
            pltpu.VMEM((n_kv - 1, seqs, 128), F32),
            pltpu.VMEM((count, n_z, PAIR, seqs, width), BF16),
            DMA((1 + 2 * count,)),
            DMA((2, n_tp - 1)),
            DMA((2, 1, n_z - 1)),
            DMA((2, 1, n_z)),
            DMA((2, n_tp - 1)),
            DMA((2, n_tp - 1)),
            DMA((2, n_kv - 1)),
            DMA((2, count)),
            DMA((2, count, n_z - 1)),
            DMA((2, count, n_z - 1)),
            DMA((2, count, n_z)),
            DMA((2, n_tp - 1)),
        ],
        compiler_params=params(collective_id=1),
        name="mix",
    )(mixed, x, cg.reshape(1, block), ow, uw, dw)
    return out, new_state


def solution(mesh):
    return jax.shard_map(
        functools.partial(fused_device, mesh.shape["kv"], mesh.shape["tp"]),
        mesh=mesh,
        in_specs=(
            P(None, ("kv", "tp")),
            P(("kv", "tp")),
            P(("kv", "tp")),
            P("kv", "tp"),
            P("kv", "tp"),
            P("kv", "tp"),
            P("kv", "tp"),
            P("tp", "kv"),
            P("kv", "tp"),
            P("tp", "kv"),
            P("kv", "tp", None, None),
        ),
        out_specs=(P(None, ("kv", "tp")), P("kv", "tp", None, None)),
        check_vma=False,
    )
```

time: 325 us -> 91.4 us (0.28)
  blocking collectives: 155 us -> 0 us
  waiting for transfers between devices: 84.5 us -> 0 us
  Pallas kernels: 0 us -> 79.2 us
  matrix products: 33.8 us -> 0 us
  other arithmetic: 29 us -> 0.01 us
  between operations: 14.6 us -> 0.67 us
  local copies, waits for them, and re-layouts: 7.43 us -> 11 us
    psum x2 -> x0, blocking collectives: 80.9 us -> none  [the longest x1 41.4 us: per_device(): totals = lax.psum(squares, ('kv', 'tp'))]
    pallas_call x0 -> x3, Pallas kernels: none -> 79.2 us  [the longest x1 44.4 us: fused_device(): pl.pallas_call(functools.partial(mix_kernel, (n_kv, n_tp, seqs, width, co...]
    all_gather x4 -> x0, blocking collectives: 73.7 us -> none  [the longest x1 31.4 us: per_device(): lax.all_gather(hidden, 'kv', axis=0, tiled=True)]
    unnamed x7 -> x0, waiting for transfers between devices: 61.2 us -> none
    dot_general x13 -> x0, matrix products: 33.8 us -> none  [the longest x2 11.5 us: retain(): jnp.einsum('shd,shde->she', query, new_state, precision=lax.Precision.HIG...]
    reduce_scatter x1 -> x0, waiting for transfers between devices: 23.3 us -> none  [per_device(): lax.psum_scatter(jnp.dot(channel_block, up_weight, preferred_element_type...]
    concatenate x2 -> x0, other arithmetic: 12 us -> none  [the longest x1 12 us: per_device(): state_out = jnp.concatenate(new_states, axis=0)]
    add x1 -> x0, other arithmetic: 9.59 us -> none  [retain(): rates[None, :, None, None] * old_state]
  transfers between devices with their start and end apart: 4 -> 0, of which waited for: 4 -> 0; matrix products, arithmetic and copies ran while one was open for 4% -> 0% of each run, Pallas kernels for 0% -> 0%
where the time goes in v1:
time: 91.4 us; the launch traced here: 90.9 us
  Pallas kernels  79.2 us (87%)
  local copies, waits for them, and re-layouts  11 us (12%)
    pallas_call x1, Pallas kernels, fused_device(): pl.pallas_call(functools.partial(mix_kernel, (n_kv, n_tp, seqs, width, co...  44.4 us
    pallas_call x1, Pallas kernels, fused_device(): pl.pallas_call(functools.partial(project_kernel, (n_kv, n_tp, seqs, width...  25.3 us
    unnamed x13, local copies, waits for them, and re-layouts  10.9 us
    pallas_call x1, Pallas kernels, fused_device(): pl.pallas_call(functools.partial(retain_kernel, heads, dk, dv), grid=(seq...  9.49 us

profile of v1, /device:TPU:0, one launch (start us, length us, event | category | flops | bytes accessed | tf_op | source)
XLA Modules:
  0.0 90.9 jit_solution(5238693918019447061)
XLA Ops:
  0.6 0.1 dynamic_slice.3.rate_ref
  0.7 25.3 %project.1 = (f32[8,1024]{1,0:T(8,128)}, f32[8,1024]{1,0:T(8,128)}, f32[8,2048]{1,0:T(8,128)}, f32[8,2048]{1,0:T(8,128)}) custom-call(bf16[64,128]{1,0:T(8,128)(2,1)} %x_ref.3, bf16[1,128]{1,0:T(2,128)(2,1)} %bitcast.2, bf16[512,1024]{1,0:T(8,128)(2,1)} %refs_0_.1, bf16[512,1024]{1,0:T(8,128)(2,1)} %refs_1_.1, bf16[512,2048]{1,0:T(8,128)(2,1)} %refs_2_.1, ...), custom_call_target="tpu_custom_call" | custom-call | tf_op jit(solution)/shard_map/project/pallas_call | solution.py:391
  26.0 0.0 copy-start
  26.0 5.8 %copy-done = f32[8,4,256,512]{3,2,1,0:T(8,128)S(1)} copy-done((f32[8,4,256,512]{3,2,1,0:T(8,128)S(1)}, f32[8,4,256,512]{3,2,1,0:T(8,128)}, u32[]{:S(2)}) %copy-start) | copy-done | bytes 16777240
  31.8 0.0 copy-start.1
  31.8 0.8 copy-done.1
  32.6 0.0 copy-start.2
  32.6 0.8 copy-done.2
  33.4 0.0 copy-start.4
  33.4 0.8 copy-done.4
  34.2 0.0 copy-start.5
  34.2 0.8 copy-done.5
  35.0 9.5 %retain.1 = (f32[8,4,256,512]{3,2,1,0:T(8,128)}, f32[8,2048]{1,0:T(8,128)S(1)}) custom-call(f32[8,1024]{1,0:T(8,128)S(1)} %copy-done.4, f32[8,1024]{1,0:T(8,128)S(1)} %copy-done.5, f32[8,2048]{1,0:T(8,128)S(1)} %copy-done.1, f32[8,2048]{1,0:T(8,128)S(1)} %copy-done.2, f32[4]{0:T(128)S(1)} %dynamic_slice.3.rate_ref, f32[8,4,256,512]{3,2,1,0:T(8,128)S(1)} %copy-done), custom_call_target="tpu_custom_call" | custom-call | tf_op jit(solution)/shard_map/retain/pallas_call | solution.py:418
  44.5 0.0 copy-start.3
  44.5 0.6 copy-done.3
  45.1 44.4 %mix.1 = bf16[64,128]{1,0:T(8,128)(2,1)} custom-call(f32[8,2048]{1,0:T(8,128)} %copy-done.3, bf16[64,128]{1,0:T(8,128)(2,1)} %x_ref.3, bf16[1,128]{1,0:T(2,128)(2,1)} %bitcast.3, bf16[2048,512]{1,0:T(8,128)(2,1)} %ow_hbm.1, bf16[512,4096]{1,0:T(8,128)(2,1)} %up_hbm.1, bf16[4096,512]{1,0:T(8,128)(2,1)} %down_hbm.1), custom_call_target="tpu_custom_call" | custom-call | tf_op jit(solution)/shard_map/mix/pallas_call | solution.py:439
  89.5 1.3 %copy.14 = bf16[64,128]{1,0:T(8,128)(2,1)} copy(bf16[64,128]{1,0:T(8,128)(2,1)} %mix.1) | data formatting | bytes 32768
  (1 shorter events, 0.0 us)
Async XLA Ops:
  26.0 5.8 %copy-start = (f32[8,4,256,512]{3,2,1,0:T(8,128)S(1)}, f32[8,4,256,512]{3,2,1,0:T(8,128)}, u32[]{:S(2)}) copy-start(f32[8,4,256,512]{3,2,1,0:T(8,128)} %old_ref.1) | copy-start | bytes 50331652
  31.8 0.8 copy-start.1
  32.6 0.8 copy-start.2
  33.4 0.8 copy-start.4
  34.2 0.8 copy-start.5
  44.5 0.6 copy-start.3
